TPU v7x, 32 devices: a whole 2x2x4 slice. The times are simulated.
32 devices in a mesh: grp: 2 (over y), fs: 4 (over z), tp: 4 (over x, core).
Axes of the slice: x: 2, y: 2, z: 4, core: 2. Of those that a mesh axis runs over, the one named last changes fastest.
Arguments:
- tokens: bfloat16 [2048, 2048], P(('grp', 'fs', 'tp')), parts along dimension 0, may hold values from -30 to 30
- gate_master: float32 [2048, 2752], P('fs', 'tp'), may hold values from -0.125 to 0.125
- up_master: float32 [2048, 2752], P('fs', 'tp'), may hold values from -0.125 to 0.125
- down_master: float32 [2048, 2752], P('fs', 'tp'), may hold values from -0.4375 to 0.4375
- norm_gain: float32 [2048], replicated, may hold values from 0.1 to 1.9
- post_gain: float32 [2048], replicated, may hold values from 0.1 to 1.9
- post_bias: float32 [2048], replicated, may hold values from -3 to 3
Outputs:
- gate_ready: bfloat16 [4096, 2752], P('grp', 'tp'), parts along dimension 0
- up_ready: bfloat16 [4096, 2752], P('grp', 'tp'), parts along dimension 0
- down_ready: bfloat16 [4096, 2752], P('grp', 'tp'), parts along dimension 0
- result: bfloat16 [2048, 2048], P(('grp', 'fs', 'tp')), parts along dimension 0
There are 2 independent parts, one for each index of `grp`. A program takes and returns all parts, laid end to end along the dimension named above; an argument that names none is the same for every part. Nothing has to cross between parts.
All inputs are finite; a program needn't handle non-finite values.
Results may differ from a plain program's by a relative error of at most 0.009.
Values may be sent and summed in bfloat16 or wider, within the bound.
A program may use at most 64 MiB of HBM per device.

v0:
```python
import jax
import jax.numpy as jnp
from jax import lax
from jax.sharding import PartitionSpec as P


def finish(wide, branch, post_gain, post_bias):
    mixed = jnp.sqrt(jnp.float32(2.0)) * wide + 0.5 * branch
    center = jnp.mean(mixed, axis=-1, keepdims=True)
    spread = jnp.mean(jnp.square(mixed - center), axis=-1, keepdims=True)
    return ((mixed - center) * lax.rsqrt(spread + 1e-05) * post_gain + post_bias).astype(
        jnp.bfloat16
    )


def local(tokens, gate_master, up_master, down_master, norm_gain, post_gain, post_bias):
    row_count = gate_master.shape[0]
    first_row = lax.axis_index("fs") * row_count
    gain_rows = lax.dynamic_slice_in_dim(norm_gain, first_row, row_count, 0)
    gate_piece = (gain_rows[:, None] * gate_master).astype(jnp.bfloat16)
    up_piece = (gain_rows[:, None] * up_master).astype(jnp.bfloat16)
    down_piece = down_master.astype(jnp.bfloat16)
    gate_ready, up_ready, down_ready = (
        lax.all_gather(gate_piece, "fs", axis=0, tiled=True),
        lax.all_gather(up_piece, "fs", axis=0, tiled=True),
        lax.all_gather(down_piece, "fs", axis=0, tiled=True),
    )
    wide = tokens.astype(jnp.float32)
    normed = (wide * lax.rsqrt(jnp.mean(wide * wide, axis=-1, keepdims=True) + 1e-06)).astype(
        jnp.bfloat16
    )
    piece = lax.all_gather(normed, "tp", axis=0, tiled=True)
    gate = jnp.dot(piece, gate_ready, preferred_element_type=jnp.float32)
    upward = jnp.dot(piece, up_ready, preferred_element_type=jnp.float32)
    hidden = (jax.nn.silu(gate) * upward).astype(jnp.bfloat16)
    branch = lax.psum_scatter(
        lax.dot_general(
            hidden, down_ready, (((1,), (1,)), ((), ())), preferred_element_type=jnp.float32
        ).astype(jnp.bfloat16),
        "tp",
        scatter_dimension=0,
        tiled=True,
    ).astype(jnp.float32)
    result = finish(wide, branch, post_gain, post_bias)
    return (gate_ready, up_ready, down_ready, result)


def solution(mesh):
    return jax.shard_map(
        local,
        mesh=mesh,
        in_specs=(
            P(("grp", "fs", "tp"), None),
            P("fs", "tp"),
            P("fs", "tp"),
            P("fs", "tp"),
            P(),
            P(),
            P(),
        ),
        out_specs=(P("grp", "tp"), P("grp", "tp"), P("grp", "tp"), P(("grp", "fs", "tp"), None)),
        check_vma=False,
    )
```

profile of v0, /device:TPU:0, one launch (start us, length us, event | category | flops | bytes accessed | tf_op | source)
XLA Modules:
  0.0 256.1 jit_solution(3088402425451007015)
XLA Ops:
  7.2 0.0 all-gather.11.cloned.1.call-start
  7.2 1.1 fusion.2
  8.3 1.8 fusion.3
  10.1 0.0 all-gather.11.cloned.1.call-update
  10.1 0.0 all-gather.5.cloned.1.call-start
  10.2 0.8 dynamic_slice.3
  10.9 0.0 copy-start.4
  10.9 3.3 %multiply_convert_fusion = (bf16[512,688]{0,1:T(8,128)(2,1)}, bf16[512,688]{0,1:T(8,128)(2,1)}) fusion(f32[512,688]{0,1:T(8,128)} %param.9, f32[512]{0:T(512)S(1)} %dynamic_slice.3, f32[512,688]{0,1:T(8,128)} %param.8), kind=kLoop, calls=%fused_computation.1 | loop fusion | flops 1409024 | bytes 4229120 | tf_op jit(solution)/shard_map/convert_element_type | solution.py:21
  14.3 0.0 all-gather.5.cloned.1.call-update
  14.3 0.0 all-gather.7.cloned.1.call-start
  14.4 0.7 all-gather.7.cloned.1.call-update
  15.1 0.0 all-gather.9.cloned.1.call-start
  15.1 0.0 copy-done.4
  15.1 0.9 convert_element_type.29
  16.1 0.0 all-gather.9.cloned.1.call-update
  16.1 0.0 reduce-scatter.2.cloned.1.call-start
  16.1 13.6 %all-gather.11.cloned.1.call-done = bf16[256,2048]{1,0:T(8,128)(2,1)} async-done(((bf16[64,2048]{1,0:T(8,128)(2,1)}), bf16[256,2048]{1,0:T(8,128)(2,1)}) %all-gather.11.cloned.1.call-update) | async-done | bytes 1048592 | tf_op jit(solution)/shard_map/all_gather | solution.py:32
  29.7 0.0 copy-start.7
  29.7 60.2 %all-gather.5.cloned.1.call-done = bf16[2048,688]{0,1:T(8,128)(2,1)} async-done(((bf16[512,688]{0,1:T(8,128)(2,1)}), bf16[2048,688]{0,1:T(8,128)(2,1)}) %all-gather.5.cloned.1.call-update) | async-done | bytes 2818064 | tf_op jit(solution)/shard_map/all_gather | solution.py:24
  89.9 3.0 %fusion.7 = f32[256,688]{0,1:T(8,128)S(1)} fusion(bf16[256,2048]{1,0:T(8,128)(2,1)} %all-gather.11.cloned.1.call-done, bf16[2048,688]{0,1:T(8,128)(2,1)} %all-gather.5.cloned.1.call-done), kind=kOutput, calls=%fused_computation.19 | convolution fusion | flops 721420288 | bytes 4571136 | tf_op jit(solution)/shard_map/dot_general | solution.py:33
  93.0 0.0 copy-start
  93.0 0.0 copy-start.5
  93.0 0.0 copy-start.6
  93.0 55.8 %all-gather.7.cloned.1.call-done = bf16[2048,688]{0,1:T(8,128)(2,1)} async-done(((bf16[512,688]{0,1:T(8,128)(2,1)}), bf16[2048,688]{0,1:T(8,128)(2,1)}) %all-gather.7.cloned.1.call-update) | async-done | bytes 2818064 | tf_op jit(solution)/shard_map/all_gather | solution.py:25
  148.8 58.8 %all-gather.9.cloned.1.call-done = bf16[2048,688]{0,1:T(8,128)(2,1)} async-done(((bf16[512,688]{0,1:T(8,128)(2,1)}), bf16[2048,688]{0,1:T(8,128)(2,1)}) %all-gather.9.cloned.1.call-update) | async-done | bytes 2818064 | tf_op jit(solution)/shard_map/all_gather | solution.py:26
  207.6 0.0 copy-done.7
  207.6 6.9 %convolution_convert_fusion = bf16[256,2048]{1,0:T(8,128)(2,1)} fusion(bf16[2048,688]{0,1:T(8,128)(2,1)} %all-gather.9.cloned.1.call-done, bf16[256,2048]{1,0:T(8,128)(2,1)S(1)} %copy-done.7, bf16[2048,688]{0,1:T(8,128)(2,1)} %all-gather.7.cloned.1.call-done, f32[256,688]{0,1:T(8,128)S(1)} %fusion.7), kind=kOutput, calls=%fused_computation | convolution fusion | flops 1444421632 | bytes 8437760 | tf_op jit(solution)/shard_map/dot_general | solution.py:37
  214.5 0.0 copy-start.1
  214.5 0.0 reduce-scatter.2.cloned.1.call-update
  214.5 23.7 %reduce-scatter.2.cloned.1.call-done = bf16[64,2048]{1,0:T(8,128)(2,1)} async-done(((bf16[256,2048]{1,0:T(8,128)(2,1)}), bf16[64,2048]{1,0:T(8,128)(2,1)}) %reduce-scatter.2.cloned.1.call-update) | async-done | bytes 262160 | tf_op jit(solution)/shard_map/reduce_scatter | solution.py:36
  238.2 0.0 copy-done
  238.2 1.2 fusion.5
  239.3 1.2 multiply_reduce_fusion
  240.5 0.0 copy-done.5
  240.6 0.0 copy-done.6
  240.6 1.8 add_convert_fusion
  242.4 0.0 copy-done.1
  242.4 0.0 copy-start.2
  242.4 1.6 copy.14
  244.0 1.3 copy-done.2
  245.2 0.0 copy-start.3
  245.2 1.6 copy.15
  246.8 1.3 copy-done.3
  248.0 1.6 copy.16
  (3 shorter events, 0.0 us)
Async XLA Ops:
  7.2 22.5 %all-gather.11.cloned.1.call-start = ((), (), s32[]{:S(2)}) async-start(), calls=%async_computation.4 | async-start | bytes 1310720 | tf_op jit(solution)/shard_map/all_gather | solution.py:32
  10.1 79.8 %all-gather.5.cloned.1.call-start = ((), (), s32[]{:S(2)}) async-start(), calls=%async_computation.1 | async-start | bytes 3522560 | tf_op jit(solution)/shard_map/all_gather | solution.py:24
  10.9 4.2 %copy-start.4 = (f32[512,688]{0,1:T(8,128)S(1)}, f32[512,688]{0,1:T(8,128)}, u32[]{:S(2)}) copy-start(f32[512,688]{0,1:T(8,128)} %param.10) | copy-start | bytes 4227076
  14.3 134.5 %all-gather.7.cloned.1.call-start = ((), (), s32[]{:S(2)}) async-start(), calls=%async_computation.2 | async-start | bytes 3522560 | tf_op jit(solution)/shard_map/all_gather | solution.py:25
  15.1 192.5 %all-gather.9.cloned.1.call-start = ((), (), s32[]{:S(2)}) async-start(), calls=%async_computation.3 | async-start | bytes 3522560 | tf_op jit(solution)/shard_map/all_gather | solution.py:26
  16.1 222.1 %reduce-scatter.2.cloned.1.call-start = ((), (), s32[]{:S(2)}) async-start(), calls=%async_computation.5 | async-start | bytes 1310720 | tf_op jit(solution)/shard_map/reduce_scatter | solution.py:36
  29.7 177.9 %copy-start.7 = (bf16[256,2048]{1,0:T(8,128)(2,1)S(1)}, bf16[256,2048]{1,0:T(8,128)(2,1)}, u32[]{:S(2)}) copy-start(bf16[256,2048]{1,0:T(8,128)(2,1)} %all-gather.11.cloned.1.call-done) | copy-start | bytes 3145732
  93.0 145.2 %copy-start = (bf16[64,2048]{1,0:T(8,128)(2,1)S(1)}, bf16[64,2048]{1,0:T(8,128)(2,1)}, u32[]{:S(2)}) copy-start(bf16[64,2048]{1,0:T(8,128)(2,1)} %param.7) | copy-start | bytes 786436
  93.0 147.6 %copy-start.5 = (f32[2048]{0:T(1024)S(1)}, f32[2048]{0:T(1024)}, u32[]{:S(2)}) copy-start(f32[2048]{0:T(1024)} %param.13) | copy-start | bytes 24580
  93.0 147.6 %copy-start.6 = (f32[2048]{0:T(1024)S(1)}, f32[2048]{0:T(1024)}, u32[]{:S(2)}) copy-start(f32[2048]{0:T(1024)} %param.12) | copy-start | bytes 24580
  214.5 27.9 %copy-start.1 = (bf16[2048,688]{0,1:T(8,128)(2,1)S(1)}, bf16[2048,688]{0,1:T(8,128)(2,1)}, u32[]{:S(2)}) copy-start(bf16[2048,688]{0,1:T(8,128)(2,1)} %all-gather.5.cloned.1.call-done) | copy-start | bytes 8454148
  242.4 2.8 %copy-start.2 = (bf16[2048,688]{0,1:T(8,128)(2,1)S(1)}, bf16[2048,688]{0,1:T(8,128)(2,1)}, u32[]{:S(2)}) copy-start(bf16[2048,688]{0,1:T(8,128)(2,1)} %all-gather.7.cloned.1.call-done) | copy-start | bytes 8454148
  245.2 2.8 %copy-start.3 = (bf16[2048,688]{0,1:T(8,128)(2,1)S(1)}, bf16[2048,688]{0,1:T(8,128)(2,1)}, u32[]{:S(2)}) copy-start(bf16[2048,688]{0,1:T(8,128)(2,1)} %all-gather.9.cloned.1.call-done) | copy-start | bytes 8454148
Sparse Core Ops, SparseCore 0:
  10.2 19.4 all-gather.10
  31.8 58.0 all-gather.4
  92.1 56.7 all-gather.6
  150.8 56.7 all-gather.8
  214.6 23.4 reduce-scatter.1
where the time goes:
time: 257 us; the launch traced here: 256 us
  waiting for transfers between devices  213 us (83%)
  between operations  13.9 us (5%)
  other arithmetic  11.4 us (4%)
  matrix products  9.93 us (4%)
  local copies, waits for them, and re-layouts  7.97 us (3%)
    all_gather x1, waiting for transfers between devices, local(): lax.all_gather(gate_piece, 'fs', axis=0, tiled=True)  60.2 us
    all_gather x1, waiting for transfers between devices, local(): lax.all_gather(down_piece, 'fs', axis=0, tiled=True)  58.8 us
    all_gather x1, waiting for transfers between devices, local(): lax.all_gather(up_piece, 'fs', axis=0, tiled=True)  55.8 us
    reduce_scatter x1, waiting for transfers between devices, local(): lax.psum_scatter(lax.dot_general(hidden, down_ready, (((1,), (1,)), ((),...  23.7 us
    all_gather x1, waiting for transfers between devices, local(): piece = lax.all_gather(normed, 'tp', axis=0, tiled=True)  13.6 us
    unnamed x19, local copies, waits for them, and re-layouts  7.21 us
    dot_general x1, matrix products, local(): lax.dot_general(hidden, down_ready, (((1,), (1,)), ((), ())), preferred_e...  6.89 us
  transfers between devices with their start and end apart: 5, of which 5 were waited for; matrix products, arithmetic and copies ran while one was open for 3% of the time, Pallas kernels for 0%

commit v1 on v0

--- a/solution.py
+++ b/solution.py
@@ -29,7 +29,12 @@
     normed = (wide * lax.rsqrt(jnp.mean(wide * wide, axis=-1, keepdims=True) + 1e-06)).astype(
         jnp.bfloat16
     )
-    piece = lax.all_gather(normed, "tp", axis=0, tiled=True)
+    ring = [normed]
+    for hop in range(3):
+        ring.append(lax.ppermute(ring[-1], "tp", [(dev, (dev + 1) % 4) for dev in range(4)]))
+    piece = jnp.roll(
+        jnp.concatenate(ring[::-1], axis=0), (lax.axis_index("tp") + 1) * ring[0].shape[0], axis=0
+    )
     gate = jnp.dot(piece, gate_ready, preferred_element_type=jnp.float32)
     upward = jnp.dot(piece, up_ready, preferred_element_type=jnp.float32)
     hidden = (jax.nn.silu(gate) * upward).astype(jnp.bfloat16)

time: 257 us -> 239 us (0.930)
  waiting for transfers between devices: 213 us -> 197 us
    ppermute x0 -> x3, waiting for transfers between devices: none -> 17.6 us  [local(): lax.ppermute(ring[-1], 'tp', [(dev, (dev + 1) % 4) for dev in range(4)])]
    all_gather x1, waiting for transfers between devices: 55.8 us -> 40.3 us  [local(): lax.all_gather(up_piece, 'fs', axis=0, tiled=True)]
    all_gather x1 -> x0, waiting for transfers between devices: 13.6 us -> none  [local(): piece = lax.all_gather(normed, 'tp', axis=0, tiled=True)]
    all_gather x1, waiting for transfers between devices: 60.2 us -> 56.2 us  [local(): lax.all_gather(gate_piece, 'fs', axis=0, tiled=True)]
    unnamed x19 -> x23, local copies, waits for them, and re-layouts: 7.21 us -> 7.31 us
  transfers between devices with their start and end apart: 5 -> 7, of which waited for: 5 -> 7; matrix products, arithmetic and copies ran while one was open for 3% -> 2% of each run, Pallas kernels for 0% -> 0%
where the time goes in v1:
time: 239 us
  waiting for transfers between devices  197 us (82%)
  between operations  13.9 us (6%)
  matrix products  9.65 us (4%)
  other arithmetic  8.98 us (4%)
  local copies, waits for them, and re-layouts  8.08 us (3%)
    all_gather x1, waiting for transfers between devices, local(): lax.all_gather(down_piece, 'fs', axis=0, tiled=True)  58.9 us
    all_gather x1, waiting for transfers between devices, local(): lax.all_gather(gate_piece, 'fs', axis=0, tiled=True)  56.2 us
    all_gather x1, waiting for transfers between devices, local(): lax.all_gather(up_piece, 'fs', axis=0, tiled=True)  40.3 us
    reduce_scatter x1, waiting for transfers between devices, local(): lax.psum_scatter(lax.dot_general(hidden, down_ready, (((1,), (1,)), ((),...  23.7 us
    ppermute x3, waiting for transfers between devices, local(): lax.ppermute(ring[-1], 'tp', [(dev, (dev + 1) % 4) for dev in range(4)])  17.6 us
    unnamed x23, local copies, waits for them, and re-layouts  7.31 us
    dot_general x1, matrix products, local(): lax.dot_general(hidden, down_ready, (((1,), (1,)), ((), ())), preferred_e...  6.93 us
  transfers between devices with their start and end apart: 7, of which 7 were waited for; matrix products, arithmetic and copies ran while one was open for 2% of the time, Pallas kernels for 0%

profile of v1, /device:TPU:0, one launch (start us, length us, event | category | flops | bytes accessed | tf_op | source)
XLA Modules:
  0.0 238.7 jit_solution(13401547003065683090)
XLA Ops:
  7.2 0.0 all-gather.6.cloned.1.call-start
  7.2 0.8 dynamic_slice.7
  8.0 0.0 copy-start.4
  8.0 3.3 %multiply_convert_fusion = (bf16[512,688]{0,1:T(8,128)(2,1)}, bf16[512,688]{0,1:T(8,128)(2,1)}) fusion(f32[512,688]{0,1:T(8,128)} %param.9, f32[512]{0:T(512)S(1)} %dynamic_slice.7, f32[512,688]{0,1:T(8,128)} %param.8), kind=kLoop, calls=%fused_computation.1 | loop fusion | flops 1409024 | bytes 4229120 | tf_op jit(solution)/shard_map/convert_element_type | solution.py:21
  11.3 0.0 copy-start
  11.3 0.0 all-gather.6.cloned.1.call-update
  11.4 0.0 all-gather.4.cloned.1.call-start
  11.4 0.7 all-gather.4.cloned.1.call-update
  12.1 0.0 all-gather.8.cloned.1.call-start
  12.2 0.0 copy-done.4
  12.2 0.9 convert_element_type.29
  13.1 0.0 all-gather.8.cloned.1.call-update
  13.1 0.0 reduce-scatter.2.cloned.1.call-start
  13.2 0.0 copy-done
  13.2 0.2 fusion.5
  13.4 0.1 fusion.6
  13.5 0.5 collective-permute-start
  14.0 6.0 %collective-permute-done = bf16[64,2048]{1,0:T(8,128)(2,1)S(1)} collective-permute-done((bf16[64,2048]{1,0:T(8,128)(2,1)S(1)}, bf16[64,2048]{1,0:T(8,128)(2,1)S(1)}, u32[]{:S(2)}, u32[]{:S(2)}) %collective-permute-start) | collective-permute-done | bytes 262176 | tf_op jit(solution)/shard_map/ppermute | solution.py:34
  20.0 0.0 collective-permute-start.1
  20.0 5.8 %collective-permute-done.1 = bf16[64,2048]{1,0:T(8,128)(2,1)S(1)} collective-permute-done((bf16[64,2048]{1,0:T(8,128)(2,1)S(1)}, bf16[64,2048]{1,0:T(8,128)(2,1)S(1)}, u32[]{:S(2)}, u32[]{:S(2)}) %collective-permute-start.1) | collective-permute-done | bytes 262176 | tf_op jit(solution)/shard_map/ppermute | solution.py:34
  25.8 0.0 collective-permute-start.2
  25.8 5.8 %collective-permute-done.2 = bf16[64,2048]{1,0:T(8,128)(2,1)S(1)} collective-permute-done((bf16[64,2048]{1,0:T(8,128)(2,1)S(1)}, bf16[64,2048]{1,0:T(8,128)(2,1)S(1)}, u32[]{:S(2)}, u32[]{:S(2)}) %collective-permute-start.2) | collective-permute-done | bytes 262176 | tf_op jit(solution)/shard_map/ppermute | solution.py:34
  31.7 0.1 constant_dynamic-update-slice_fusion.4
  31.9 0.1 constant_dynamic-update-slice_fusion
  32.0 40.3 %all-gather.6.cloned.1.call-done = bf16[2048,688]{0,1:T(8,128)(2,1)} async-done(((bf16[512,688]{0,1:T(8,128)(2,1)}), bf16[2048,688]{0,1:T(8,128)(2,1)}) %all-gather.6.cloned.1.call-update) | async-done | bytes 2818064 | tf_op jit(solution)/shard_map/all_gather | solution.py:25
  72.3 2.7 %fusion = f32[256,688]{0,1:T(8,128)S(1)} fusion(bf16[2048,688]{0,1:T(8,128)(2,1)} %all-gather.6.cloned.1.call-done, bf16[512,2048]{1,0:T(8,128)(2,1)S(1)} %constant_dynamic-update-slice_fusion, s32[]{:T(128)S(6)} %select_n.18), kind=kOutput, calls=%fused_computation.3 | convolution fusion | flops 721420288 | bytes 4571140 | tf_op jit(solution)/shard_map/dot_general | solution.py:39
  75.0 56.2 %all-gather.4.cloned.1.call-done = bf16[2048,688]{0,1:T(8,128)(2,1)} async-done(((bf16[512,688]{0,1:T(8,128)(2,1)}), bf16[2048,688]{0,1:T(8,128)(2,1)}) %all-gather.4.cloned.1.call-update) | async-done | bytes 2818064 | tf_op jit(solution)/shard_map/all_gather | solution.py:24
  131.2 58.9 %all-gather.8.cloned.1.call-done = bf16[2048,688]{0,1:T(8,128)(2,1)} async-done(((bf16[512,688]{0,1:T(8,128)(2,1)}), bf16[2048,688]{0,1:T(8,128)(2,1)}) %all-gather.8.cloned.1.call-update) | async-done | bytes 2818064 | tf_op jit(solution)/shard_map/all_gather | solution.py:26
  190.1 0.0 copy-start.5
  190.1 0.0 copy-start.6
  190.1 6.9 %convolution_convert_fusion = bf16[256,2048]{1,0:T(8,128)(2,1)} fusion(bf16[2048,688]{0,1:T(8,128)(2,1)} %all-gather.8.cloned.1.call-done, f32[256,688]{0,1:T(8,128)S(1)} %fusion, bf16[2048,688]{0,1:T(8,128)(2,1)} %all-gather.4.cloned.1.call-done, bf16[512,2048]{1,0:T(8,128)(2,1)S(1)} %constant_dynamic-update-slice_fusion, s32[]{:T(128)S(6)} %select_n.18), kind=kOutput, calls=%fused_computation | convolution fusion | flops 1444421632 | bytes 8437764 | tf_op jit(solution)/shard_map/dot_general | solution.py:42
  197.0 0.0 copy-start.2
  197.0 0.0 reduce-scatter.2.cloned.1.call-update
  197.0 23.7 %reduce-scatter.2.cloned.1.call-done = bf16[64,2048]{1,0:T(8,128)(2,1)} async-done(((bf16[256,2048]{1,0:T(8,128)(2,1)}), bf16[64,2048]{1,0:T(8,128)(2,1)}) %reduce-scatter.2.cloned.1.call-update) | async-done | bytes 262160 | tf_op jit(solution)/shard_map/reduce_scatter | solution.py:41
  220.7 1.2 fusion.12
  221.9 1.2 multiply_reduce_fusion
  223.1 0.0 copy-done.5
  223.1 0.0 copy-done.6
  223.1 1.8 add_convert_fusion
  224.9 0.0 copy-done.2
  224.9 0.0 copy-start.1
  224.9 1.6 copy.21
  226.5 1.3 copy-done.1
  227.8 0.0 copy-start.3
  227.8 1.6 copy.22
  229.3 1.3 copy-done.3
  230.6 1.6 copy.23
  (9 shorter events, 0.1 us)
Async XLA Ops:
  7.2 65.1 %all-gather.6.cloned.1.call-start = ((), (), s32[]{:S(2)}) async-start(), calls=%async_computation.2 | async-start | bytes 3522560 | tf_op jit(solution)/shard_map/all_gather | solution.py:25
  8.0 4.2 %copy-start.4 = (f32[512,688]{0,1:T(8,128)S(1)}, f32[512,688]{0,1:T(8,128)}, u32[]{:S(2)}) copy-start(f32[512,688]{0,1:T(8,128)} %param.10) | copy-start | bytes 4227076
  11.3 1.9 copy-start
  11.4 119.8 %all-gather.4.cloned.1.call-start = ((), (), s32[]{:S(2)}) async-start(), calls=%async_computation.1 | async-start | bytes 3522560 | tf_op jit(solution)/shard_map/all_gather | solution.py:24
  12.1 178.0 %all-gather.8.cloned.1.call-start = ((), (), s32[]{:S(2)}) async-start(), calls=%async_computation.3 | async-start | bytes 3522560 | tf_op jit(solution)/shard_map/all_gather | solution.py:26
  13.1 207.6 %reduce-scatter.2.cloned.1.call-start = ((), (), s32[]{:S(2)}) async-start(), calls=%async_computation.4 | async-start | bytes 1310720 | tf_op jit(solution)/shard_map/reduce_scatter | solution.py:41
  13.5 6.5 %collective-permute-start = (bf16[64,2048]{1,0:T(8,128)(2,1)S(1)}, bf16[64,2048]{1,0:T(8,128)(2,1)S(1)}, u32[]{:S(2)}, u32[]{:S(2)}) collective-permute-start(bf16[64,2048]{1,0:T(8,128)(2,1)S(1)} %fusion.6), channel_id=1, source_target_pairs={{0,1},{1,2},{2,3},{3,0},{4,5},{5,6},{6,7},{7,4},{8,9},{9,10},{10,1... | collective-permute-start | bytes 786440 | tf_op jit(solution)/shard_map/ppermute | solution.py:34
  20.0 5.8 %collective-permute-start.1 = (bf16[64,2048]{1,0:T(8,128)(2,1)S(1)}, bf16[64,2048]{1,0:T(8,128)(2,1)S(1)}, u32[]{:S(2)}, u32[]{:S(2)}) collective-permute-start(bf16[64,2048]{1,0:T(8,128)(2,1)S(1)} %collective-permute-done), channel_id=1, source_target_pairs={{0,1},{1,2},{2,3},{3,0},{4,5},{5,6},{6,7},{7,4},{8,9},{9,10},{10,1... | collective-permute-start | bytes 786440 | tf_op jit(solution)/shard_map/ppermute | solution.py:34
  25.8 5.8 %collective-permute-start.2 = (bf16[64,2048]{1,0:T(8,128)(2,1)S(1)}, bf16[64,2048]{1,0:T(8,128)(2,1)S(1)}, u32[]{:S(2)}, u32[]{:S(2)}) collective-permute-start(bf16[64,2048]{1,0:T(8,128)(2,1)S(1)} %collective-permute-done.1), channel_id=1, source_target_pairs={{0,1},{1,2},{2,3},{3,0},{4,5},{5,6},{6,7},{7,4},{8,9},{9,10},{10,1... | collective-permute-start | bytes 786440 | tf_op jit(solution)/shard_map/ppermute | solution.py:34
  190.1 33.0 %copy-start.5 = (f32[2048]{0:T(1024)S(1)}, f32[2048]{0:T(1024)}, u32[]{:S(2)}) copy-start(f32[2048]{0:T(1024)} %param.13) | copy-start | bytes 24580
  190.1 33.0 %copy-start.6 = (f32[2048]{0:T(1024)S(1)}, f32[2048]{0:T(1024)}, u32[]{:S(2)}) copy-start(f32[2048]{0:T(1024)} %param.12) | copy-start | bytes 24580
  197.0 27.9 %copy-start.2 = (bf16[2048,688]{0,1:T(8,128)(2,1)S(1)}, bf16[2048,688]{0,1:T(8,128)(2,1)}, u32[]{:S(2)}) copy-start(bf16[2048,688]{0,1:T(8,128)(2,1)} %all-gather.4.cloned.1.call-done) | copy-start | bytes 8454148
  224.9 2.8 %copy-start.1 = (bf16[2048,688]{0,1:T(8,128)(2,1)S(1)}, bf16[2048,688]{0,1:T(8,128)(2,1)}, u32[]{:S(2)}) copy-start(bf16[2048,688]{0,1:T(8,128)(2,1)} %all-gather.6.cloned.1.call-done) | copy-start | bytes 8454148
  227.8 2.8 %copy-start.3 = (bf16[2048,688]{0,1:T(8,128)(2,1)S(1)}, bf16[2048,688]{0,1:T(8,128)(2,1)}, u32[]{:S(2)}) copy-start(bf16[2048,688]{0,1:T(8,128)(2,1)} %all-gather.8.cloned.1.call-done) | copy-start | bytes 8454148
Sparse Core Ops, SparseCore 0:
  11.5 60.7 all-gather.5
  74.4 56.7 all-gather.3
  133.3 56.7 all-gather.7
  197.2 23.4 reduce-scatter.1
